TPU v7x, 32 devices: a whole 2x2x4 slice. The times are simulated.
32 devices in a mesh: sp: 8 (over z, y), tp: 4 (over x, core).
Axes of the slice: x: 2, y: 2, z: 4, core: 2. Of those that a mesh axis runs over, the one named last changes fastest.
Arguments:
- hidden_states: bfloat16 [4096, 4096], P('sp', 'tp'), may hold values from -6 to 6
- pre_gain: float32 [2, 4096], replicated, may hold values from 0.1 to 1.9
- post_gain: float32 [2, 4096], P(None, 'tp'), may hold values from 0.1 to 1.9
- w_value: bfloat16 [2, 4096, 2048], P(None, 'sp', 'tp'), may hold values from -0.09375 to 0.09375
- w_outer: bfloat16 [2, 4096, 2048], P(None, 'sp', 'tp'), may hold values from -0.09375 to 0.09375
- w_inner: bfloat16 [2, 4096, 2048], P(None, 'sp', 'tp'), may hold values from -0.09375 to 0.09375
- taps: float32 [2, 3, 2048], P(None, None, 'tp'), may hold values from -3 to 3
- w_out: bfloat16 [2, 2048, 4096], P(None, 'tp', 'sp'), as said below
Outputs:
- final_states: bfloat16 [4096, 4096], P('sp', 'tp')
Inputs may be any that keep to these rules, and one draw needn't show every extreme that they name: `w_out`: independent entries; the columns fall into 8 groups of 512 consecutive columns, each group with its own scale.
All inputs are finite; a program needn't handle non-finite values.
Results may differ from a plain program's by a relative error of at most 0.024.
Values may be sent and summed in bfloat16 or wider, within the bound.
A program may use at most 128 MiB of HBM per device.

v0:
```python
import jax
import jax.numpy as jnp
from jax import lax
from jax.sharding import PartitionSpec as P

D = 4096
eps = 1e-06


def passed_along(value, axis, by):
    size = lax.axis_size(axis)
    pairs = [(i, i + by) for i in range(size) if 0 <= i + by < size]
    return lax.ppermute(value, axis, pairs)


def local(hidden_states, pre_gain, post_gain, w_value, w_outer, w_inner, taps, w_out):
    current = hidden_states
    layers = w_value.shape[0]
    whole_value, whole_outer, whole_inner, whole_out = (
        lax.all_gather(w_value, "sp", axis=1, tiled=True),
        lax.all_gather(w_outer, "sp", axis=1, tiled=True),
        lax.all_gather(w_inner, "sp", axis=1, tiled=True),
        lax.all_gather(w_out, "sp", axis=2, tiled=True),
    )
    for layer_index in range(layers):
        gathered = lax.all_gather(current, "tp", axis=1, tiled=True)
        widened = gathered.astype(jnp.float32)
        normed = (
            widened
            * lax.rsqrt(jnp.mean(widened * widened, axis=1, keepdims=True) + eps)
            * pre_gain[layer_index]
        ).astype(jnp.bfloat16)
        value_proj = jnp.dot(normed, whole_value[layer_index], preferred_element_type=jnp.float32)
        outer_proj = jnp.dot(normed, whole_outer[layer_index], preferred_element_type=jnp.float32)
        inner_proj = jnp.dot(normed, whole_inner[layer_index], preferred_element_type=jnp.float32)
        gated_input = (inner_proj * value_proj).astype(jnp.bfloat16)
        before = passed_along(gated_input[-2:], "sp", 1)
        extended = jnp.concatenate([before, gated_input], axis=0).astype(jnp.float32)
        length = gated_input.shape[0]
        kernel = taps[layer_index]
        convolved = (
            extended[0:length] * kernel[0]
            + extended[1 : length + 1] * kernel[1]
            + extended[2 : length + 2] * kernel[2]
        )
        conv_out = (outer_proj * convolved).astype(jnp.bfloat16)
        partial_terms = jnp.dot(
            conv_out, whole_out[layer_index], preferred_element_type=jnp.float32
        )
        mixed = lax.psum_scatter(
            partial_terms.astype(jnp.bfloat16), "tp", scatter_dimension=1, tiled=True
        ).astype(jnp.float32)
        power = lax.psum(jnp.sum(mixed * mixed, axis=1), "tp")
        rescale = lax.rsqrt(power / D + eps)
        current = (
            current.astype(jnp.float32) + mixed * rescale[:, None] * post_gain[layer_index]
        ).astype(jnp.bfloat16)
    return current


def solution(mesh):
    placed = (
        P("sp", "tp"),
        P(),
        P(None, "tp"),
        P(None, "sp", "tp"),
        P(None, "sp", "tp"),
        P(None, "sp", "tp"),
        P(None, None, "tp"),
        P(None, "tp", "sp"),
    )
    return jax.shard_map(
        local, mesh=mesh, in_specs=placed, out_specs=P("sp", "tp"), check_vma=False
    )
```

profile of v0, /device:TPU:0, one launch (start us, length us, event | category | flops | bytes accessed | tf_op | source)
XLA Modules:
  0.0 729.6 jit_solution(7224380522898905791)
XLA Ops:
  6.5 0.7 all-gather.7.cloned.1.call-update
  7.3 0.0 all-gather.13.cloned.1.call-start
  7.3 0.7 all-gather.13.cloned.1.call-update
  8.0 0.0 all-gather.11.cloned.1.call-start
  8.1 0.7 all-gather.11.cloned.1.call-update
  8.7 0.0 all-gather.9.cloned.1.call-start
  8.8 0.5 all-gather.9.cloned.1.call-update
  9.3 0.0 all-gather.15.cloned.1.call-start
  9.4 0.5 all-gather.15.cloned.1.call-update
  9.9 0.0 reduce-scatter.3.cloned.1.call-start
  10.0 36.1 %all-gather.7.cloned.1.call-done = bf16[512,4096]{1,0:T(8,128)(2,1)} async-done(((bf16[512,1024]{1,0:T(8,128)(2,1)}), bf16[512,4096]{1,0:T(8,128)(2,1)}) %all-gather.7.cloned.1.call-update) | async-done | bytes 4194320 | tf_op jit(solution)/shard_map/all_gather | solution.py:26
  46.1 3.1 fusion
  49.2 123.6 %all-gather.13.cloned.1.call-done = bf16[2,4096,512]{2,1,0:T(8,128)(2,1)} async-done(((bf16[2,512,512]{2,1,0:T(8,128)(2,1)}), bf16[2,4096,512]{2,1,0:T(8,128)(2,1)}) %all-gather.13.cloned.1.call-update) | async-done | bytes 8388624 | tf_op jit(solution)/shard_map/all_gather | solution.py:20
  172.8 5.8 fusion.9
  178.6 119.0 %all-gather.11.cloned.1.call-done = bf16[2,4096,512]{2,1,0:T(8,128)(2,1)} async-done(((bf16[2,512,512]{2,1,0:T(8,128)(2,1)}), bf16[2,4096,512]{2,1,0:T(8,128)(2,1)}) %all-gather.11.cloned.1.call-update) | async-done | bytes 8388624 | tf_op jit(solution)/shard_map/all_gather | solution.py:22
  297.6 5.8 fusion.26
  303.5 2.5 collective-permute-start
  306.0 1.3 collective-permute-done
  307.3 0.2 maximum_convert_fusion
  307.4 114.9 %all-gather.9.cloned.1.call-done = bf16[2,4096,512]{2,1,0:T(8,128)(2,1)} async-done(((bf16[2,512,512]{2,1,0:T(8,128)(2,1)}), bf16[2,4096,512]{2,1,0:T(8,128)(2,1)}) %all-gather.9.cloned.1.call-update) | async-done | bytes 8388624 | tf_op jit(solution)/shard_map/all_gather | solution.py:21
  422.4 6.0 fusion.27
  428.4 119.0 %all-gather.15.cloned.1.call-done = bf16[2,512,4096]{2,1,0:T(8,128)(2,1)} async-done(((bf16[2,512,512]{2,1,0:T(8,128)(2,1)}), bf16[2,512,4096]{2,1,0:T(8,128)(2,1)}) %all-gather.15.cloned.1.call-update) | async-done | bytes 8388624 | tf_op jit(solution)/shard_map/all_gather | solution.py:23
  547.4 6.7 convolution_convert_fusion.1
  554.1 0.0 reduce-scatter.3.cloned.1.call-update
  554.1 0.0 all-gather.17.cloned.1.call-start
  554.1 0.6 copy-done.5
  554.8 42.1 %reduce-scatter.3.cloned.1.call-done = bf16[512,1024]{1,0:T(8,128)(2,1)} async-done(((bf16[512,4096]{1,0:T(8,128)(2,1)}), bf16[512,1024]{1,0:T(8,128)(2,1)}) %reduce-scatter.3.cloned.1.call-update) | async-done | bytes 1048592 | tf_op jit(solution)/shard_map/reduce_scatter | solution.py:50
  596.8 1.5 fusion.12
  598.3 5.8 psum.14
  604.1 2.6 fusion.15
  606.7 0.0 all-gather.17.cloned.1.call-update
  606.8 0.2 reduce-scatter.5.cloned.1.call-start
  607.0 35.0 %all-gather.17.cloned.1.call-done = bf16[512,4096]{1,0:T(8,128)(2,1)} async-done(((bf16[512,1024]{1,0:T(8,128)(2,1)}), bf16[512,4096]{1,0:T(8,128)(2,1)}) %all-gather.17.cloned.1.call-update) | async-done | bytes 4194320 | tf_op jit(solution)/shard_map/all_gather | solution.py:26
  642.0 3.2 fusion.3
  645.2 0.2 copy-done.1
  645.4 4.7 fusion.6
  650.2 4.7 fusion.24
  655.0 3.4 collective-permute-start.1
  658.3 1.3 collective-permute-done.1
  659.6 0.2 maximum_convert_fusion.1
  659.8 2.6 fusion.25
  662.4 0.7 slice-done.1
  663.2 4.3 convolution_convert_fusion
  667.5 0.0 reduce-scatter.5.cloned.1.call-update
  667.5 45.4 %reduce-scatter.5.cloned.1.call-done = bf16[512,1024]{1,0:T(8,128)(2,1)} async-done(((bf16[512,4096]{1,0:T(8,128)(2,1)}), bf16[512,1024]{1,0:T(8,128)(2,1)}) %reduce-scatter.5.cloned.1.call-update) | async-done | bytes 1048592 | tf_op jit(solution)/shard_map/reduce_scatter | solution.py:50
  712.9 1.5 fusion.16
  714.4 5.8 psum.15
  720.1 2.6 fusion.19
  (29 shorter events, 0.1 us)
Async XLA Ops:
  6.5 3.4 copy-start.3
  6.5 39.6 %all-gather.7.cloned.1.call-start = ((), (), s32[]{:S(2)}) async-start(), calls=%async_computation.2 | async-start | bytes 5242880 | tf_op jit(solution)/shard_map/all_gather | solution.py:26
  7.3 165.5 %all-gather.13.cloned.1.call-start = ((), (), s32[]{:S(2)}) async-start(), calls=%async_computation.5 | async-start | bytes 9437184 | tf_op jit(solution)/shard_map/all_gather | solution.py:20
  8.0 289.6 %all-gather.11.cloned.1.call-start = ((), (), s32[]{:S(2)}) async-start(), calls=%async_computation.4 | async-start | bytes 9437184 | tf_op jit(solution)/shard_map/all_gather | solution.py:22
  8.7 413.6 %all-gather.9.cloned.1.call-start = ((), (), s32[]{:S(2)}) async-start(), calls=%async_computation.3 | async-start | bytes 9437184 | tf_op jit(solution)/shard_map/all_gather | solution.py:21
  9.3 538.1 %all-gather.15.cloned.1.call-start = ((), (), s32[]{:S(2)}) async-start(), calls=%async_computation.6 | async-start | bytes 9437184 | tf_op jit(solution)/shard_map/all_gather | solution.py:23
  9.9 586.9 %reduce-scatter.3.cloned.1.call-start = ((), (), s32[]{:S(2)}) async-start(), calls=%async_computation.7 | async-start | bytes 5242880 | tf_op jit(solution)/shard_map/reduce_scatter | solution.py:50
  178.6 127.4 %copy-start.4 = (f32[2,3,512]{2,0,1:T(2,128)S(1)}, f32[2,3,512]{2,0,1:T(2,128)}, u32[]{:S(2)}) copy-start(f32[2,3,512]{2,0,1:T(2,128)} %param.14) | copy-start | bytes 36868
  303.5 3.8 collective-permute-start
  554.1 0.7 copy-start.5
  554.1 50.0 %copy-start.2 = (bf16[512,1024]{1,0:T(8,128)(2,1)S(1)}, bf16[512,1024]{1,0:T(8,128)(2,1)}, u32[]{:S(2)}) copy-start(bf16[512,1024]{1,0:T(8,128)(2,1)} %param.8) | copy-start | bytes 3145732
  554.1 87.9 %all-gather.17.cloned.1.call-start = ((), (), s32[]{:S(2)}) async-start(), calls=%async_computation.8 | async-start | bytes 5242880 | tf_op jit(solution)/shard_map/all_gather | solution.py:26
  606.8 106.1 %reduce-scatter.5.cloned.1.call-start = ((), (), s32[]{:S(2)}) async-start(), calls=%async_computation.9 | async-start | bytes 5242880 | tf_op jit(solution)/shard_map/reduce_scatter | solution.py:50
  642.0 3.4 copy-start.1
  645.4 14.4 %slice-start.2 = ((s8[8388608]{0:T(1024)(128)(4,1)}), s8[4194304]{0:T(1024)(128)(4,1)S(1)}, s32[]{:S(2)}) async-start(s8[8388608]{0:T(1024)(128)(4,1)} %bitcast.68), calls=%async_computation.12 | async-start | bytes 8388608
  650.2 9.6 %slice-start.3 = ((s8[8388608]{0:T(1024)(128)(4,1)}), s8[4194304]{0:T(1024)(128)(4,1)S(1)}, s32[]{:S(2)}) async-start(s8[8388608]{0:T(1024)(128)(4,1)} %bitcast.68), calls=%async_computation.13 | async-start | bytes 8388608
  655.0 4.7 collective-permute-start.1
  659.6 2.8 slice-start
  659.8 3.3 slice-start.1
  667.5 52.7 %copy-start = (bf16[512,1024]{1,0:T(8,128)(2,1)S(1)}, bf16[512,1024]{1,0:T(8,128)(2,1)}, u32[]{:S(2)}) copy-start(bf16[512,1024]{1,0:T(8,128)(2,1)} %fusion.15) | copy-start | bytes 3145732
Sparse Core Ops, SparseCore 0:
  8.9 37.1 all-gather.6
  48.3 124.4 all-gather.12
  175.0 122.6 all-gather.10
  299.7 122.6 all-gather.8
  424.2 123.1 all-gather.14
  554.2 42.5 reduce-scatter.2
  606.9 35.0 all-gather.16
  667.6 45.2 reduce-scatter.4
where the time goes:
time: 730 us
  waiting for transfers between devices  641 us (88%)
  matrix products  40.7 us (6%)
  other arithmetic  14.9 us (2%)
  between operations  13.7 us (2%)
  blocking collectives  11.5 us (2%)
    all_gather x1, waiting for transfers between devices, local(): lax.all_gather(w_value, 'sp', axis=1, tiled=True)  124 us
    all_gather x1, waiting for transfers between devices, local(): lax.all_gather(w_out, 'sp', axis=2, tiled=True)  119 us
    all_gather x1, waiting for transfers between devices, local(): lax.all_gather(w_inner, 'sp', axis=1, tiled=True)  119 us
    all_gather x1, waiting for transfers between devices, local(): lax.all_gather(w_outer, 'sp', axis=1, tiled=True)  115 us
    reduce_scatter x2, waiting for transfers between devices, local(): lax.psum_scatter(partial_terms.astype(jnp.bfloat16), 'tp', scatter_dimens...  87.4 us
    all_gather x2, waiting for transfers between devices, local(): gathered = lax.all_gather(current, 'tp', axis=1, tiled=True)  71.1 us
  transfers between devices with their start and end apart: 10, of which 10 were waited for; matrix products, arithmetic and copies ran while one was open for 3% of the time, Pallas kernels for 0%

commit v1 on v0

--- a/solution.py
+++ b/solution.py
@@ -17,7 +17,7 @@
     current = hidden_states
     layers = w_value.shape[0]
     whole_value, whole_outer, whole_inner, whole_out = (
-        lax.all_gather(w_value, "sp", axis=1, tiled=True),
+        jnp.concatenate(lax.all_gather(w_value, "sp"), axis=1),
         lax.all_gather(w_outer, "sp", axis=1, tiled=True),
         lax.all_gather(w_inner, "sp", axis=1, tiled=True),
         lax.all_gather(w_out, "sp", axis=2, tiled=True),

time: 730 us -> 730 us (level)
  no operation moved by 1% of the time
where the time goes in v1:
time: 730 us; the launch traced here: 729 us
  waiting for transfers between devices  638 us (87%)
  matrix products  37.2 us (5%)
  other arithmetic  14.9 us (2%)
  between operations  13.7 us (2%)
  blocking collectives  11.5 us (2%)
  local copies, waits for them, and re-layouts  7.81 us (1%)
    all_gather x1, waiting for transfers between devices, local(): lax.all_gather(w_value, 'sp')  124 us
    all_gather x1, waiting for transfers between devices, local(): lax.all_gather(w_out, 'sp', axis=2, tiled=True)  119 us
    all_gather x1, waiting for transfers between devices, local(): lax.all_gather(w_inner, 'sp', axis=1, tiled=True)  116 us
    all_gather x1, waiting for transfers between devices, local(): lax.all_gather(w_outer, 'sp', axis=1, tiled=True)  115 us
    reduce_scatter x2, waiting for transfers between devices, local(): lax.psum_scatter(partial_terms.astype(jnp.bfloat16), 'tp', scatter_dimens...  87.4 us
    all_gather x2, waiting for transfers between devices, local(): gathered = lax.all_gather(current, 'tp', axis=1, tiled=True)  71.1 us
  transfers between devices with their start and end apart: 10, of which 10 were waited for; matrix products, arithmetic and copies ran while one was open for 3% of the time, Pallas kernels for 0%

profile of v1, /device:TPU:0, one launch (start us, length us, event | category | flops | bytes accessed | tf_op | source)
XLA Modules:
  0.0 729.5 jit_solution(13753367195559894327)
XLA Ops:
  6.5 0.7 all-gather.8.cloned.1.call-update
  7.3 0.0 all-gather.18.cloned.1.call-start
  7.3 0.7 all-gather.18.cloned.1.call-update
  8.0 0.0 all-gather.12.cloned.1.call-start
  8.1 0.7 all-gather.12.cloned.1.call-update
  8.7 0.0 all-gather.10.cloned.1.call-start
  8.8 0.5 all-gather.10.cloned.1.call-update
  9.3 0.0 all-gather.14.cloned.1.call-start
  9.4 0.5 all-gather.14.cloned.1.call-update
  9.9 0.0 reduce-scatter.3.cloned.1.call-start
  10.0 36.1 %all-gather.8.cloned.1.call-done = bf16[512,4096]{1,0:T(8,128)(2,1)} async-done(((bf16[512,1024]{1,0:T(8,128)(2,1)}), bf16[512,4096]{1,0:T(8,128)(2,1)}) %all-gather.8.cloned.1.call-update) | async-done | bytes 4194320 | tf_op jit(solution)/shard_map/all_gather | solution.py:26
  46.1 3.1 fusion
  49.2 123.5 %all-gather.18.cloned.1.call-done = bf16[16,512,512]{2,1,0:T(8,128)(2,1)} async-done(((bf16[2,512,512]{2,1,0:T(8,128)(2,1)}), bf16[16,512,512]{2,1,0:T(8,128)(2,1)}) %all-gather.18.cloned.1.call-update) | async-done | bytes 8388624 | tf_op jit(solution)/shard_map/all_gather | solution.py:20
  172.7 5.3 fusion.38
  178.0 0.9 copy-done.1
  178.9 2.4 fusion.34
  181.3 116.3 %all-gather.12.cloned.1.call-done = bf16[2,4096,512]{2,1,0:T(8,128)(2,1)} async-done(((bf16[2,512,512]{2,1,0:T(8,128)(2,1)}), bf16[2,4096,512]{2,1,0:T(8,128)(2,1)}) %all-gather.12.cloned.1.call-update) | async-done | bytes 8388624 | tf_op jit(solution)/shard_map/all_gather | solution.py:22
  297.6 5.8 fusion.24
  303.5 2.5 collective-permute-start
  306.0 1.3 collective-permute-done
  307.2 0.2 maximum_convert_fusion
  307.4 114.9 %all-gather.10.cloned.1.call-done = bf16[2,4096,512]{2,1,0:T(8,128)(2,1)} async-done(((bf16[2,512,512]{2,1,0:T(8,128)(2,1)}), bf16[2,4096,512]{2,1,0:T(8,128)(2,1)}) %all-gather.10.cloned.1.call-update) | async-done | bytes 8388624 | tf_op jit(solution)/shard_map/all_gather | solution.py:21
  422.3 6.0 fusion.25
  428.3 119.0 %all-gather.14.cloned.1.call-done = bf16[2,512,4096]{2,1,0:T(8,128)(2,1)} async-done(((bf16[2,512,512]{2,1,0:T(8,128)(2,1)}), bf16[2,512,4096]{2,1,0:T(8,128)(2,1)}) %all-gather.14.cloned.1.call-update) | async-done | bytes 8388624 | tf_op jit(solution)/shard_map/all_gather | solution.py:23
  547.4 6.6 convolution_convert_fusion.1
  553.9 0.0 reduce-scatter.3.cloned.1.call-update
  553.9 0.0 all-gather.16.cloned.1.call-start
  554.0 0.6 copy-done.6
  554.6 42.1 %reduce-scatter.3.cloned.1.call-done = bf16[512,1024]{1,0:T(8,128)(2,1)} async-done(((bf16[512,4096]{1,0:T(8,128)(2,1)}), bf16[512,1024]{1,0:T(8,128)(2,1)}) %reduce-scatter.3.cloned.1.call-update) | async-done | bytes 1048592 | tf_op jit(solution)/shard_map/reduce_scatter | solution.py:50
  596.7 1.5 fusion.10
  598.2 5.8 psum.14
  604.0 2.6 fusion.13
  606.6 0.2 reduce-scatter.5.cloned.1.call-start
  606.9 35.0 %all-gather.16.cloned.1.call-done = bf16[512,4096]{1,0:T(8,128)(2,1)} async-done(((bf16[512,1024]{1,0:T(8,128)(2,1)}), bf16[512,4096]{1,0:T(8,128)(2,1)}) %all-gather.16.cloned.1.call-update) | async-done | bytes 4194320 | tf_op jit(solution)/shard_map/all_gather | solution.py:26
  641.8 3.2 fusion.3
  645.1 0.2 copy-done.2
  645.3 4.7 fusion.30
  650.1 4.7 fusion.22
  654.8 3.4 collective-permute-start.1
  658.2 1.3 collective-permute-done.1
  659.5 0.2 maximum_convert_fusion.1
  659.7 2.6 fusion.23
  662.3 0.7 slice-done.1
  663.0 4.3 convolution_convert_fusion
  667.3 45.4 %reduce-scatter.5.cloned.1.call-done = bf16[512,1024]{1,0:T(8,128)(2,1)} async-done(((bf16[512,4096]{1,0:T(8,128)(2,1)}), bf16[512,1024]{1,0:T(8,128)(2,1)}) %reduce-scatter.5.cloned.1.call-update) | async-done | bytes 1048592 | tf_op jit(solution)/shard_map/reduce_scatter | solution.py:50
  712.7 1.5 fusion.14
  714.2 5.8 psum.15
  720.0 2.6 fusion.17
  (32 shorter events, 0.2 us)
Async XLA Ops:
  6.5 3.4 copy-start.4
  6.5 39.6 %all-gather.8.cloned.1.call-start = ((), (), s32[]{:S(2)}) async-start(), calls=%async_computation.2 | async-start | bytes 5242880 | tf_op jit(solution)/shard_map/all_gather | solution.py:26
  7.3 165.5 %all-gather.18.cloned.1.call-start = ((), (), s32[]{:S(2)}) async-start(), calls=%async_computation.9 | async-start | bytes 9437184 | tf_op jit(solution)/shard_map/all_gather | solution.py:20
  8.0 289.6 %all-gather.12.cloned.1.call-start = ((), (), s32[]{:S(2)}) async-start(), calls=%async_computation.4 | async-start | bytes 9437184 | tf_op jit(solution)/shard_map/all_gather | solution.py:22
  8.7 413.6 %all-gather.10.cloned.1.call-start = ((), (), s32[]{:S(2)}) async-start(), calls=%async_computation.3 | async-start | bytes 9437184 | tf_op jit(solution)/shard_map/all_gather | solution.py:21
  9.3 538.0 %all-gather.14.cloned.1.call-start = ((), (), s32[]{:S(2)}) async-start(), calls=%async_computation.5 | async-start | bytes 9437184 | tf_op jit(solution)/shard_map/all_gather | solution.py:23
  9.9 586.8 %reduce-scatter.3.cloned.1.call-start = ((), (), s32[]{:S(2)}) async-start(), calls=%async_computation.6 | async-start | bytes 5242880 | tf_op jit(solution)/shard_map/reduce_scatter | solution.py:50
  172.7 6.2 copy-start.1
  181.3 124.6 %copy-start.5 = (f32[2,3,512]{2,0,1:T(2,128)S(1)}, f32[2,3,512]{2,0,1:T(2,128)}, u32[]{:S(2)}) copy-start(f32[2,3,512]{2,0,1:T(2,128)} %param.14) | copy-start | bytes 36868
  303.5 3.8 collective-permute-start
  553.9 0.7 copy-start.6
  553.9 50.0 %copy-start.3 = (bf16[512,1024]{1,0:T(8,128)(2,1)S(1)}, bf16[512,1024]{1,0:T(8,128)(2,1)}, u32[]{:S(2)}) copy-start(bf16[512,1024]{1,0:T(8,128)(2,1)} %param.8) | copy-start | bytes 3145732
  553.9 87.9 %all-gather.16.cloned.1.call-start = ((), (), s32[]{:S(2)}) async-start(), calls=%async_computation.7 | async-start | bytes 5242880 | tf_op jit(solution)/shard_map/all_gather | solution.py:26
  606.6 106.1 %reduce-scatter.5.cloned.1.call-start = ((), (), s32[]{:S(2)}) async-start(), calls=%async_computation.8 | async-start | bytes 5242880 | tf_op jit(solution)/shard_map/reduce_scatter | solution.py:50
  641.8 3.4 copy-start.2
  645.3 14.4 %slice-start.2 = ((s8[8388608]{0:T(1024)(128)(4,1)}), s8[4194304]{0:T(1024)(128)(4,1)S(1)}, s32[]{:S(2)}) async-start(s8[8388608]{0:T(1024)(128)(4,1)} %bitcast.72), calls=%async_computation.12 | async-start | bytes 8388608
  650.0 9.6 %slice-start.3 = ((s8[8388608]{0:T(1024)(128)(4,1)}), s8[4194304]{0:T(1024)(128)(4,1)S(1)}, s32[]{:S(2)}) async-start(s8[8388608]{0:T(1024)(128)(4,1)} %bitcast.72), calls=%async_computation.13 | async-start | bytes 8388608
  654.8 4.7 collective-permute-start.1
  659.5 2.8 slice-start
  659.7 3.3 slice-start.1
  667.3 52.7 %copy-start = (bf16[512,1024]{1,0:T(8,128)(2,1)S(1)}, bf16[512,1024]{1,0:T(8,128)(2,1)}, u32[]{:S(2)}) copy-start(bf16[512,1024]{1,0:T(8,128)(2,1)} %fusion.13) | copy-start | bytes 3145732
Sparse Core Ops, SparseCore 0:
  8.9 37.1 all-gather.7
  48.2 124.4 all-gather.17
  174.9 122.6 all-gather.11
  299.6 122.6 all-gather.9
  424.2 123.1 all-gather.13
  554.1 42.5 reduce-scatter.2
  606.7 35.0 all-gather.15
  667.4 45.2 reduce-scatter.4
